TPU v7x, 32 devices: a whole 2x2x4 slice. The times are simulated.
32 devices in a mesh: sp: 16 (over z, y, x), tp: 2 (over core).
Axes of the slice: x: 2, y: 2, z: 4, core: 2. Of those that a mesh axis runs over, the one named last changes fastest.
Arguments:
- tokens: bfloat16 [4096, 2048], P('sp', 'tp'), may hold values from -6 to 6
- norm_gain: float32 [2048], replicated, may hold values from 0.1 to 1.9
- query_weight: bfloat16 [2048, 1024], P(None, 'tp'), may hold values from -0.18782524 to 0.18782524
- key_weight: bfloat16 [2048, 1024], P(None, 'tp'), may hold values from -0.18782524 to 0.18782524
- value_weight: bfloat16 [2048, 1024], P(None, 'tp'), may hold values from -0.125 to 0.125
- gate_weight: bfloat16 [2048, 1024], P(None, 'tp'), may hold values from -0.125 to 0.125
- outer_weight: bfloat16 [2048, 1024], P(None, 'tp'), may hold values from -0.125 to 0.125
- inner_weight: bfloat16 [2048, 1024], P(None, 'tp'), may hold values from -0.125 to 0.125
- signal_weight: bfloat16 [2048, 1024], P(None, 'tp'), may hold values from -0.125 to 0.125
- conv_taps: float32 [3, 1024], P(None, 'tp'), may hold values from -3.5 to 3.5
- lambdas: float32 [8], P('tp'), may hold values from 0.3 to 0.8
- head_gain: float32 [1024], P('tp'), may hold values from 0.1 to 1.9
- attn_out_weight: bfloat16 [1024, 2048], P('tp'), may hold values from -0.125 to 0.125
- conv_out_weight: bfloat16 [1024, 2048], P('tp'), may hold values from -0.125 to 0.125
Outputs:
- mixed: bfloat16 [4096, 2048], P(('sp', 'tp'))
- log_totals: float32 [8, 2, 4096], P('tp', None, 'sp')
All inputs are finite; a program needn't handle non-finite values.
Results may differ from a plain program's by a relative error of at most 0.014.
Values may be sent and summed in bfloat16 or wider, within the bound.
A program may use at most 128 MiB of HBM per device.

v0:
```python
import jax
import jax.numpy as jnp
from jax import lax
from jax.sharding import PartitionSpec as P


def passed_along(shard, axis, by):
    count = lax.axis_size(axis)
    pairs = [(i, i + by) for i in range(count) if 0 <= i + by < count]
    return lax.ppermute(shard, axis, pairs)


def per_device(
    tokens,
    norm_gain,
    query_weight,
    key_weight,
    value_weight,
    gate_weight,
    outer_weight,
    inner_weight,
    signal_weight,
    conv_taps,
    lambdas,
    head_gain,
    attn_out_weight,
    conv_out_weight,
):
    row_count = tokens.shape[0]
    width = norm_gain.shape[0]
    weights = [
        query_weight,
        key_weight,
        value_weight,
        gate_weight,
        outer_weight,
        inner_weight,
        signal_weight,
    ]
    splits = []
    running = 0
    for weight in weights[:-1]:
        running = running + weight.shape[1]
        splits.append(running)
    joined = jnp.concatenate(weights, axis=1)
    empty = jnp.zeros((row_count, joined.shape[1]), jnp.float32)
    piece = lax.all_gather(tokens, "tp", axis=1, tiled=True)
    summed = empty
    piece_f = piece.astype(jnp.float32)
    normed_piece = (piece.astype(jnp.float32) * norm_gain).astype(jnp.bfloat16)
    raw = jnp.dot(normed_piece, joined, preferred_element_type=jnp.float32)
    squares = jnp.sum(piece_f * piece_f, axis=-1)
    scale = lax.rsqrt(squares / width + 1e-06)
    projected = (raw * scale[:, None]).astype(jnp.bfloat16)
    query, key, value, attn_gate, outer, inner, signal = jnp.split(projected, splits, axis=1)
    head_count = lambdas.shape[0]
    key_size = query_weight.shape[1] // (head_count * 2)
    value_size = value_weight.shape[1] // head_count
    score_scale = key_size ** (-0.5)
    own_index = lax.axis_index("sp")
    local_pos = jnp.arange(row_count, dtype=jnp.int32)
    query_parts = [query]
    position_parts = [own_index * row_count + local_pos]
    query_parts = [
        segment.reshape(segment.shape[0], head_count, 2, key_size) for segment in query_parts
    ]

    def absorb(current, query_rows, row_pos, key_block, value_block, key_pos):
        running_max, summed, accum = current
        score = (
            jnp.einsum("qhmd,khmd->hmqk", query_rows, key_block, preferred_element_type=jnp.float32)
            * score_scale
        )
        visible = row_pos[:, None] >= key_pos[None, :]
        masked = jnp.where(visible, score, -1e30)
        new_max = jnp.maximum(running_max, jnp.max(masked, axis=-1, keepdims=True))
        weights_now = jnp.where(visible, jnp.exp(masked - new_max), 0.0)
        factor = jnp.exp(running_max - new_max)
        summed = summed * factor + jnp.sum(weights_now, axis=-1, keepdims=True)
        accum = accum * factor + jnp.einsum(
            "hmqk,khd->hmqd",
            weights_now.astype(jnp.bfloat16),
            value_block,
            preferred_element_type=jnp.float32,
        )
        return (new_max, summed, accum)

    def fresh(rows):
        return (
            jnp.full((head_count, 2, rows, 1), -1e30, jnp.float32),
            jnp.zeros((head_count, 2, rows, 1), jnp.float32),
            jnp.zeros((head_count, 2, rows, value_size), jnp.float32),
        )

    start_states = tuple((fresh(segment.shape[0]) for segment in query_parts))
    carry = start_states
    key_piece = lax.all_gather(key, "sp", axis=0, tiled=True)
    value_piece = lax.all_gather(value, "sp", axis=0, tiled=True)
    length = key_piece.shape[0]
    block_len = 512
    key_blocks = key_piece.reshape(length // block_len, block_len, head_count, 2, key_size)
    value_blocks = value_piece.reshape(length // block_len, block_len, head_count, value_size)

    def one_block(states, item):
        key_block, value_block, block_id = item
        first_key = block_id * block_len
        key_pos = first_key + jnp.arange(block_len, dtype=jnp.int32)
        updated = []
        for current, query_rows, row_pos in zip(states, query_parts, position_parts):

            def compute(held, query_rows=query_rows, row_pos=row_pos):
                return absorb(held, query_rows, row_pos, key_block, value_block, key_pos)

            def unchanged(held):
                return held

            updated.append(
                lax.cond(first_key <= row_pos[row_pos.shape[0] - 1], compute, unchanged, current)
            )
        return (tuple(updated), None)

    carry, _ = lax.scan(
        one_block,
        carry,
        (key_blocks, value_blocks, jnp.arange(length // block_len, dtype=jnp.int32)),
    )
    states = carry
    running_max = jnp.concatenate([held[0] for held in states], axis=2)
    summed = jnp.concatenate([held[1] for held in states], axis=2)
    accum = jnp.concatenate([held[2] for held in states], axis=2)
    mapped = accum / summed
    diff = mapped[:, 0] - lambdas[:, None, None] * mapped[:, 1]
    log_totals = jnp.log(summed[..., 0]) + running_max[..., 0]
    diff = jnp.transpose(diff, (1, 0, 2))
    normed = (
        diff
        * lax.rsqrt(jnp.mean(diff * diff, axis=-1, keepdims=True) + 1e-05)
        * head_gain.reshape(head_count, value_size)
    )
    normed = normed.reshape(row_count, head_count * value_size)
    head_out = (normed * jax.nn.silu(attn_gate.astype(jnp.float32))).astype(jnp.bfloat16)
    taps = conv_taps.shape[0]
    inner_sig = (inner.astype(jnp.float32) * signal.astype(jnp.float32)).astype(jnp.bfloat16)
    before = passed_along(inner_sig[row_count - (taps - 1) :], "sp", 1)
    extended = jnp.concatenate([before, inner_sig], axis=0).astype(jnp.float32)
    convolved = jnp.zeros((row_count, inner_sig.shape[1]), jnp.float32)
    for position in range(taps):
        convolved = convolved + conv_taps[position] * extended[position : position + row_count]
    conv_out = (outer.astype(jnp.float32) * convolved).astype(jnp.bfloat16)
    mixed = lax.psum_scatter(
        (
            jnp.dot(head_out, attn_out_weight, preferred_element_type=jnp.float32)
            + jnp.dot(conv_out, conv_out_weight, preferred_element_type=jnp.float32)
        ).astype(jnp.bfloat16),
        "tp",
        scatter_dimension=0,
        tiled=True,
    )
    return (mixed, log_totals)


def solution(mesh):
    placed = (
        P("sp", "tp"),
        P(),
        P(None, "tp"),
        P(None, "tp"),
        P(None, "tp"),
        P(None, "tp"),
        P(None, "tp"),
        P(None, "tp"),
        P(None, "tp"),
        P(None, "tp"),
        P("tp"),
        P("tp"),
        P("tp", None),
        P("tp", None),
    )
    return jax.shard_map(
        per_device,
        mesh=mesh,
        in_specs=placed,
        out_specs=(P(("sp", "tp"), None), P("tp", None, "sp")),
        check_vma=False,
    )
```

profile of v0, /device:TPU:0, one launch (start us, length us, event | category | flops | bytes accessed | tf_op | source)
XLA Modules:
  0.0 289.5 jit_solution(3425671837255536505)
XLA Ops:
  7.2 0.7 all-gather.4.cloned.1.call-update
  8.0 3.2 %constant_dynamic-update-slice_fusion.6 = bf16[2048,3584]{1,0:T(8,128)(2,1)} fusion(bf16[2048,512]{1,0:T(8,128)(2,1)} %param.20), kind=kLoop, calls=%fused_computation.70 | loop fusion | bytes 4194304
  11.2 1.5 constant_dynamic-update-slice_fusion.5
  12.7 1.5 constant_dynamic-update-slice_fusion.4
  14.3 1.5 constant_dynamic-update-slice_fusion.3
  15.8 1.5 constant_dynamic-update-slice_fusion.2
  17.3 1.5 constant_dynamic-update-slice_fusion.1
  18.8 1.5 constant_dynamic-update-slice_fusion
  20.4 0.9 all-gather.4.cloned.1.call-done
  21.3 1.5 fusion.23
  22.9 9.5 %fusion.20 = bf16[256,3584]{1,0:T(8,128)(2,1)S(1)} fusion(bf16[2048,3584]{1,0:T(8,128)(2,1)} %constant_dynamic-update-slice_fusion, f32[256]{0:T(256)S(1)} %add_rsqrt_fusion.1, bf16[256,2048]{1,0:T(8,128)(2,1)} %all-gather.4.cloned.1.call-done, f32[2048]{0:T(1024)S(1)} %copy-done.12), kind=kOutput, calls=%fused_computation.25 | convolution fusion | flops 3761504256 | bytes 17572864 | tf_op jit(solution)/shard_map/dot_general | solution.py:51
  32.3 1.2 copy-done.9
  33.6 0.8 fusion.48
  34.5 0.7 all-gather.8.cloned.1.call-update
  35.3 1.1 multiply_convert_fusion
  36.4 4.1 %collective-permute-start = (bf16[2,512]{1,0:T(2,128)(2,1)S(1)}, bf16[2,512]{1,0:T(2,128)(2,1)S(1)}, u32[]{:S(2)}, u32[]{:S(2)}) collective-permute-start(bf16[2,512]{1,0:T(2,128)(2,1)S(1)} %slice.41), channel_id=1, source_target_pairs={{0,2},{2,4},{4,6},{6,8},{8,10},{10,12},{12,14},{14,16},{16,18},{18... | collective-permute-start | bytes 6152 | tf_op jit(solution)/shard_map/ppermute | solution.py:10
  40.6 1.0 collective-permute-done
  41.6 0.9 maximum_convert_fusion
  42.5 69.5 %all-gather.6.cloned.1.call-done = bf16[4096,512]{1,0:T(8,128)(2,1)} async-done(((bf16[256,512]{1,0:T(8,128)(2,1)}), bf16[4096,512]{1,0:T(8,128)(2,1)}) %all-gather.6.cloned.1.call-update) | async-done | bytes 4194320 | tf_op jit(solution)/shard_map/all_gather | solution.py:97
  112.0 16.1 %reshape.41 = bf16[8,512,4,2,64]{4,3,2,1,0:T(2,128)(2,1)} reshape(bf16[4096,512]{1,0:T(8,128)(2,1)} %all-gather.6.cloned.1.call-done) | data formatting | bytes 8388608 | tf_op jit(solution)/shard_map/reshape | solution.py:101
  128.1 20.1 %copy.25 = bf16[8,512,4,2,64]{1,4,3,2,0:T(8,128)(2,1)} copy(bf16[8,512,4,2,64]{4,3,2,1,0:T(2,128)(2,1)} %reshape.41) | data formatting | bytes 8388608 | tf_op jit(solution)/shard_map/while | solution.py:122
  148.1 41.4 %all-gather.8.cloned.1.call-done = bf16[4096,512]{1,0:T(8,128)(2,1)} async-done(((bf16[256,512]{1,0:T(8,128)(2,1)}), bf16[4096,512]{1,0:T(8,128)(2,1)}) %all-gather.8.cloned.1.call-update) | async-done | bytes 4194320 | tf_op jit(solution)/shard_map/all_gather | solution.py:98
  189.6 6.9 %reshape.38 = bf16[8,512,4,128]{3,2,1,0:T(4,128)(2,1)} reshape(bf16[4096,512]{1,0:T(8,128)(2,1)} %all-gather.8.cloned.1.call-done) | data formatting | bytes 8388608 | tf_op jit(solution)/shard_map/reshape | solution.py:102
  196.5 5.2 %copy.26 = bf16[8,512,4,128]{3,1,2,0:T(8,128)(2,1)} copy(bf16[8,512,4,128]{3,2,1,0:T(4,128)(2,1)} %reshape.38) | data formatting | bytes 8388608 | tf_op jit(solution)/shard_map/while | solution.py:122
  201.8 27.3 %while.14 = (s32[]{:T(128)}, f32[4,2,256,1]{2,1,0,3:T(2,128)S(1)}, f32[4,2,256,1]{2,1,0,3:T(2,128)S(1)}, f32[4,2,256,128]{3,2,1,0:T(8,128)S(1)}, s32[8]{0:T(128)...) while((s32[]{:T(128)}, f32[4,2,256,1]{2,1,0,3:T(2,128)S(1)}, ...), condition=%wide.region_6.7_spmd, body=%wide.region_1.6_spmd.sunk | while | flops 416946688 | bytes 16656687 | solution.py:122
  201.8 0.7 dynamic_slice.33
  203.1 0.6 slice.89
  204.4 5.9 %conditional.2 = ((f32[4,2,256,1]{2,1,0,3:T(2,128)S(1)}, f32[4,2,256,1]{2,1,0,3:T(2,128)S(1)}, f32[4,2,256,128]{3,2,1,0:T(8,128)S(1)})) conditional(s32[]{:T(128)} %convert_element_type.98, (f32[4,2,256,1]{2,1,0,3:T(2,128)S(1)}, f32[4,2,256,1]{2,1,0,3:T(2,128)S(1)}, f32[4,2,256,128]{3,2,1,0:T(8,128)S(1)}) %tuple.43, (s32[256]{0:T(256)S(1)}, ...), branch_computations={%region_2.2_spmd, %region_3.5_spmd} | conditional | flops 416946688 | bytes 16654372 | solution.py:118
  204.6 1.9 fusion
  206.5 1.0 fusion.2
  207.6 2.8 fusion.6
  210.4 0.7 dynamic_slice.33
  211.7 0.6 slice.89
  213.1 0.7 dynamic_slice.33
  214.4 0.6 slice.89
  215.7 0.7 dynamic_slice.33
  217.1 0.6 slice.89
  218.4 0.7 dynamic_slice.33
  219.7 0.6 slice.89
  221.1 0.7 dynamic_slice.33
  222.4 0.6 slice.89
  223.7 0.7 dynamic_slice.33
  225.1 0.6 slice.89
  226.4 0.7 dynamic_slice.33
  227.7 0.6 slice.89
  229.8 1.9 fusion.38
  231.7 2.8 fusion.21
  235.1 47.8 %reduce-scatter.2.cloned.1.call-done = bf16[128,2048]{1,0:T(8,128)(2,1)} async-done(((bf16[256,2048]{1,0:T(8,128)(2,1)}), bf16[128,2048]{1,0:T(8,128)(2,1)}) %reduce-scatter.2.cloned.1.call-update) | async-done | bytes 524304 | tf_op jit(solution)/shard_map/reduce_scatter | solution.py:150
  (66 shorter events, 2.1 us)
Async XLA Ops:
  7.2 222.6 %copy-start = (bf16[512,2048]{1,0:T(8,128)(2,1)S(1)}, bf16[512,2048]{1,0:T(8,128)(2,1)}, u32[]{:S(2)}) copy-start(bf16[512,2048]{1,0:T(8,128)(2,1)} %param.30) | copy-start | bytes 6291460
  7.2 14.1 %all-gather.4.cloned.1.call-start = ((), (), s32[]{:S(2)}) async-start(), calls=%async_computation.1 | async-start | bytes 1572864 | tf_op jit(solution)/shard_map/all_gather | solution.py:47
  7.9 104.1 %all-gather.6.cloned.1.call-start = ((), (), s32[]{:S(2)}) async-start(), calls=%async_computation.2 | async-start | bytes 4456448 | tf_op jit(solution)/shard_map/all_gather | solution.py:97
  8.0 3.2 %copy-start.3 = (bf16[2048,512]{1,0:T(8,128)(2,1)S(1)}, bf16[2048,512]{1,0:T(8,128)(2,1)}, u32[]{:S(2)}) copy-start(bf16[2048,512]{1,0:T(8,128)(2,1)} %param.21) | copy-start | bytes 6291460
  8.0 4.8 %copy-start.4 = (bf16[2048,512]{1,0:T(8,128)(2,1)S(1)}, bf16[2048,512]{1,0:T(8,128)(2,1)}, u32[]{:S(2)}) copy-start(bf16[2048,512]{1,0:T(8,128)(2,1)} %param.22) | copy-start | bytes 6291460
  11.2 3.1 %copy-start.5 = (bf16[2048,512]{1,0:T(8,128)(2,1)S(1)}, bf16[2048,512]{1,0:T(8,128)(2,1)}, u32[]{:S(2)}) copy-start(bf16[2048,512]{1,0:T(8,128)(2,1)} %param.23) | copy-start | bytes 6291460
  12.7 3.0 %copy-start.6 = (bf16[2048,512]{1,0:T(8,128)(2,1)S(1)}, bf16[2048,512]{1,0:T(8,128)(2,1)}, u32[]{:S(2)}) copy-start(bf16[2048,512]{1,0:T(8,128)(2,1)} %param.24) | copy-start | bytes 6291460
  14.3 3.0 %copy-start.7 = (bf16[2048,512]{1,0:T(8,128)(2,1)S(1)}, bf16[2048,512]{1,0:T(8,128)(2,1)}, u32[]{:S(2)}) copy-start(bf16[2048,512]{1,0:T(8,128)(2,1)} %param.25) | copy-start | bytes 6291460
  15.8 3.1 %copy-start.8 = (bf16[2048,512]{1,0:T(8,128)(2,1)S(1)}, bf16[2048,512]{1,0:T(8,128)(2,1)}, u32[]{:S(2)}) copy-start(bf16[2048,512]{1,0:T(8,128)(2,1)} %param.26) | copy-start | bytes 6291460
  17.3 5.5 %copy-start.12 = (f32[2048]{0:T(1024)S(1)}, f32[2048]{0:T(1024)}, u32[]{:S(2)}) copy-start(f32[2048]{0:T(1024)} %param.19) | copy-start | bytes 24580
  22.8 12.4 %copy-start.10 = (f32[3,512]{1,0:T(4,128)S(1)}, f32[3,512]{1,0:T(4,128)}, u32[]{:S(2)}) copy-start(f32[3,512]{1,0:T(4,128)} %param.27) | copy-start | bytes 18436
  32.3 1.2 copy-start.9
  34.4 155.1 %all-gather.8.cloned.1.call-start = ((), (), s32[]{:S(2)}) async-start(), calls=%async_computation.3 | async-start | bytes 4456448 | tf_op jit(solution)/shard_map/all_gather | solution.py:98
  35.2 247.8 %reduce-scatter.2.cloned.1.call-start = ((), (), s32[]{:S(2)}) async-start(), calls=%async_computation.4 | async-start | bytes 1572864 | tf_op jit(solution)/shard_map/reduce_scatter | solution.py:150
  36.4 5.2 %collective-permute-start = (bf16[2,512]{1,0:T(2,128)(2,1)S(1)}, bf16[2,512]{1,0:T(2,128)(2,1)S(1)}, u32[]{:S(2)}, u32[]{:S(2)}) collective-permute-start(bf16[2,512]{1,0:T(2,128)(2,1)S(1)} %slice.41), channel_id=1, source_target_pairs={{0,2},{2,4},{4,6},{6,8},{8,10},{10,12},{12,14},{14,16},{16,18},{18... | collective-permute-start | bytes 6152 | tf_op jit(solution)/shard_map/ppermute | solution.py:10
  201.8 27.7 %copy-start.11 = (f32[4]{0:T(128)S(1)}, f32[4]{0:T(128)}, u32[]{:S(2)}) copy-start(f32[4]{0:T(128)} %param.28) | copy-start | bytes 52
  201.8 28.0 %copy-start.13 = (f32[512]{0:T(512)S(1)}, f32[512]{0:T(512)}, u32[]{:S(2)}) copy-start(f32[512]{0:T(512)} %param.29) | copy-start | bytes 6148
  229.1 2.6 copy-start.1
  229.1 2.6 copy-start.2
Sparse Core Ops, SparseCore 0:
  9.5 11.7 all-gather.3
  34.6 77.3 all-gather.5
  115.3 74.1 all-gather.7
  234.6 48.2 reduce-scatter.1
where the time goes:
time: 292 us; the launch traced here: 289 us
  waiting for transfers between devices  162 us (55%)
  local copies, waits for them, and re-layouts  73.4 us (25%)
  matrix products  18.8 us (6%)
  between operations  14 us (5%)
  loops' own time  11 us (4%)
  other arithmetic  5.93 us (2%)
  starting transfers between devices  4.27 us (1%)
    all_gather x1, waiting for transfers between devices, per_device(): key_piece = lax.all_gather(key, 'sp', axis=0, tiled=True)  69.5 us
    reduce_scatter x1, waiting for transfers between devices, per_device(): lax.psum_scatter((jnp.dot(head_out, attn_out_weight, preferred_element_ty...  47.8 us
    all_gather x1, waiting for transfers between devices, per_device(): value_piece = lax.all_gather(value, 'sp', axis=0, tiled=True)  41.4 us
    while x2, local copies, waits for them, and re-layouts, per_device(): lax.scan(one_block, carry, (key_blocks, value_blocks, jnp.arange(length /...  25.2 us
    reshape x1, local copies, waits for them, and re-layouts, per_device(): key_piece.reshape(length // block_len, block_len, head_count, 2, key_size)  16.1 us
    unnamed x34, local copies, waits for them, and re-layouts  12.1 us
    another operation x1, loops' own time, per_device(): lax.scan(one_block, carry, (key_blocks, value_blocks, jnp.arange(length /...  10.8 us
    dot_general x1, matrix products, per_device(): raw = jnp.dot(normed_piece, joined, preferred_element_type=jnp.float32)  9.46 us
  transfers between devices with their start and end apart: 5, of which 5 were waited for; matrix products, arithmetic and copies ran while one was open for 18% of the time, Pallas kernels for 0%

commit v1 on v0

--- a/solution.py
+++ b/solution.py
@@ -1,7 +1,14 @@
+import functools
+import math
+
 import jax
 import jax.numpy as jnp
 from jax import lax
+from jax.experimental import pallas as pl
+from jax.experimental.pallas import tpu as pltpu
 from jax.sharding import PartitionSpec as P
+
+MESH = pl.DeviceIdType.MESH
 
 
 def passed_along(shard, axis, by):
@@ -159,6 +166,448 @@
     return (mixed, log_totals)
 
 
+RELAY = 4
+
+
+def fused_kernel(
+    sp_count,
+    heads,
+    tokens_ref,
+    gain_ref,
+    wq_hbm,
+    wk_hbm,
+    wv_hbm,
+    wg_hbm,
+    wouter_hbm,
+    winner_hbm,
+    wsignal_hbm,
+    taps_ref,
+    lambdas_ref,
+    head_gain_ref,
+    wo_hbm,
+    wc_hbm,
+    mixed_ref,
+    totals_ref,
+    other_tokens,
+    normed,
+    w_vmem,
+    wo_vmem,
+    wc_vmem,
+    kv_send,
+    q_send,
+    kv_all,
+    q_all,
+    row_max,
+    accum,
+    gate,
+    outer,
+    inner_sig,
+    tail_in,
+    extended,
+    conv_out,
+    head_out,
+    conv_part,
+    o_send,
+    o_all,
+    lt_send,
+    lt_all,
+    part_send,
+    part_recv,
+    w_sem,
+    tok_sem,
+    tail_sem,
+    part_sem,
+    stage_s,
+    stage_r,
+    q_s,
+    q_r,
+    x_s,
+    x_r,
+    y_s,
+    y_r,
+    dx_s,
+    dx_r,
+    dy_s,
+    dy_r,
+    o_s,
+    o_r,
+    lt_s,
+    lt_r,
+    local_sem,
+):
+    rows, half = tokens_ref.shape
+    width = 2 * half
+    local = wq_hbm.shape[1]
+    lanes = local // heads
+    s = lax.axis_index("sp")
+    t = lax.axis_index("tp")
+    plane = s // RELAY
+    member = lax.rem(s, RELAY)
+    right_in_pair = member + 1 - 2 * lax.rem(member, 2)
+    across = lax.rem(member + 2, RELAY)
+    x_dev = plane * RELAY + right_in_pair
+    y_dev = plane * RELAY + across
+    following = lax.rem(s + 1, sp_count)
+    preceding = lax.rem(s + sp_count - 1, sp_count)
+
+    def at(sp_index, tp_index=None):
+        return {"sp": sp_index, "tp": t if tp_index is None else tp_index}
+
+    def remote(src, dst, send_sem, recv_sem, device):
+        return pltpu.make_async_remote_copy(
+            src_ref=src,
+            dst_ref=dst,
+            send_sem=send_sem,
+            recv_sem=recv_sem,
+            device_id=device,
+            device_id_type=MESH,
+        )
+
+    sources = [wk_hbm, wv_hbm, wq_hbm, winner_hbm, wsignal_hbm, wouter_hbm, wg_hbm]
+    weight_copies = [
+        pltpu.make_async_copy(ref, w_vmem.at[i], w_sem.at[i]) for i, ref in enumerate(sources)
+    ]
+    weight_copies.append(pltpu.make_async_copy(wc_hbm, wc_vmem, w_sem.at[len(sources)]))
+    weight_copies.append(pltpu.make_async_copy(wo_hbm, wo_vmem, w_sem.at[len(sources) + 1]))
+    for copy in weight_copies:
+        copy.start()
+
+    barrier = pltpu.get_barrier_semaphore()
+    greeted = [at(s, 1 - t), at(x_dev), at(y_dev), at(following), at(preceding)]
+    for step in range(1, heads):
+        greeted.append(at(lax.rem(plane + step, heads) * RELAY + member))
+    for device in greeted:
+        pl.semaphore_signal(barrier, inc=1, device_id=device, device_id_type=MESH)
+    pl.semaphore_wait(barrier, len(greeted))
+
+    tokens_out = remote(tokens_ref, other_tokens, tok_sem.at[0], tok_sem.at[1], at(s, 1 - t))
+    tokens_out.start()
+
+    row_max[...] = jnp.full(row_max.shape, -1e30, jnp.float32)
+    accum[...] = jnp.zeros(accum.shape, jnp.float32)
+
+    mine = pl.ds(pl.multiple_of(t * half, half), half)
+    theirs = pl.ds(pl.multiple_of((1 - t) * half, half), half)
+    own_f = tokens_ref[...].astype(jnp.float32)
+    squares = jnp.sum(own_f * own_f, axis=-1, keepdims=True)
+    normed[:, mine] = (own_f * gain_ref[:, mine]).astype(jnp.bfloat16)
+    tokens_out.wait()
+    other_f = other_tokens[...].astype(jnp.float32)
+    squares = squares + jnp.sum(other_f * other_f, axis=-1, keepdims=True)
+    normed[:, theirs] = (other_f * gain_ref[:, theirs]).astype(jnp.bfloat16)
+    scale = lax.rsqrt(squares / width + 1e-06)
+
+    def project(index):
+        weight_copies[index].wait()
+        raw = jnp.dot(normed[...], w_vmem[index], preferred_element_type=jnp.float32)
+        return (raw * scale).astype(jnp.bfloat16)
+
+    for index in range(2):
+        projected = project(index)
+        for h in range(heads):
+            kv_send[h, :, index * lanes : (index + 1) * lanes] = projected[
+                :, h * lanes : (h + 1) * lanes
+            ]
+
+    started = []
+
+    def launch(copy):
+        copy.start()
+        started.append(copy)
+
+    def block(plane_index, place):
+        return kv_all.at[plane_index * RELAY + place]
+
+    keep = pltpu.make_async_copy(kv_send.at[plane], kv_all.at[s], local_sem.at[0])
+    keep.start()
+    own_block = kv_send.at[plane]
+    launch(remote(own_block, kv_all.at[s], x_s.at[0], x_r.at[plane], at(x_dev)))
+    launch(remote(own_block, kv_all.at[s], y_s.at[0], y_r.at[plane], at(y_dev)))
+    for step in range(1, heads):
+        target = lax.rem(plane + step, heads)
+        launch(
+            remote(
+                kv_send.at[target],
+                kv_all.at[s],
+                stage_s.at[step],
+                stage_r.at[plane],
+                at(target * RELAY + member),
+            )
+        )
+
+    projected = project(2)
+    for h in range(heads):
+        q_send[h] = projected[:, h * lanes : (h + 1) * lanes]
+    keep_q = pltpu.make_async_copy(q_send.at[plane], q_all.at[plane], local_sem.at[1])
+    keep_q.start()
+    q_copies = []
+    for step in range(1, heads):
+        target = lax.rem(plane + step, heads)
+        q_copy = remote(
+            q_send.at[target],
+            q_all.at[plane],
+            q_s.at[step],
+            q_r.at[plane],
+            at(target * RELAY + member),
+        )
+        launch(q_copy)
+
+    inner = project(3).astype(jnp.float32)
+    signal = project(4).astype(jnp.float32)
+    inner_sig[...] = (inner * signal).astype(jnp.bfloat16)
+    tail = tail_in.shape[0]
+    launch(
+        remote(
+            inner_sig.at[pl.ds(rows - tail, tail)],
+            tail_in,
+            tail_sem.at[0],
+            tail_sem.at[1],
+            at(following),
+        )
+    )
+
+    order = [plane] + [k + jnp.where(plane <= k, 1, 0) for k in range(heads - 1)]
+    half_rows = rows // 2
+    first_half, second_half = pl.ds(0, half_rows), pl.ds(half_rows, half_rows)
+
+    def arrived(dst, recv_sem):
+        remote(dst, dst, stage_s.at[0], recv_sem, at(x_dev)).wait_recv()
+
+    def forward_stage(k):
+        c = order[k]
+        here = block(c, member)
+        arrived(here, stage_r.at[c])
+        launch(remote(here, here, x_s.at[k], x_r.at[c], at(x_dev)))
+        launch(remote(here, here, y_s.at[k], y_r.at[c], at(y_dev)))
+
+    def forward_square(k):
+        c = order[k]
+        from_x = block(c, right_in_pair)
+        arrived(from_x, x_r.at[c])
+        piece = from_x.at[first_half]
+        launch(remote(piece, piece, dy_s.at[k], dy_r.at[c], at(y_dev)))
+        from_y = block(c, across)
+        arrived(from_y, y_r.at[c])
+        piece = from_y.at[second_half]
+        launch(remote(piece, piece, dx_s.at[k], dx_r.at[c], at(x_dev)))
+
+    def finish_plane(k):
+        c = order[k]
+        diagonal = block(c, RELAY - 1 - member)
+        arrived(diagonal.at[first_half], dy_r.at[c])
+        arrived(diagonal.at[second_half], dx_r.at[c])
+
+    exponent = (lanes // 2) ** (-0.5) * math.log2(math.e)
+    span = RELAY * rows
+    lane = lax.broadcasted_iota(jnp.int32, (1, lanes), 1)
+
+    def attend(qi, c, masked):
+        held = kv_all[pl.ds(c * RELAY, RELAY)].reshape(span, 2 * lanes)
+        keys = held[:, :lanes]
+        values = jnp.concatenate(
+            [held[:, lanes:], jnp.ones((span, lanes), jnp.bfloat16)], axis=1
+        )
+        both = q_all[qi]
+        for m in range(2):
+            of_map = (lane < lanes // 2) if m == 0 else (lane >= lanes // 2)
+            query = both * of_map.astype(jnp.float32).astype(jnp.bfloat16)
+            score = (
+                lax.dot_general(
+                    query, keys, (((1,), (1,)), ((), ())), preferred_element_type=jnp.float32
+                )
+                * exponent
+            )
+            if masked:
+                row = lax.broadcasted_iota(jnp.int32, (rows, span), 0) + member * rows
+                col = lax.broadcasted_iota(jnp.int32, (rows, span), 1)
+                score = jnp.where(row >= col, score, -1e30)
+            before = row_max[2 * qi + m]
+            top = jnp.maximum(before, jnp.max(score, axis=-1, keepdims=True))
+            weights = jnp.exp2(score - top[:, :1]).astype(jnp.bfloat16)
+            factor = jnp.exp2(before - top)[:, :1]
+            row_max[2 * qi + m] = top
+            accum[2 * qi + m] = accum[2 * qi + m] * factor + jnp.dot(
+                weights, values, preferred_element_type=jnp.float32
+            )
+
+    def attend_plane(k):
+        c = order[k]
+        attend(c, c, True)
+
+        for qi in range(1, heads):
+
+            @pl.when(qi > c)
+            def _(qi=qi):
+                attend(qi, c, False)
+
+    forward_stage(1)
+    forward_square(0)
+    outer[...] = project(5)
+    gate[...] = project(6)
+
+    arrived(tail_in, tail_sem.at[1])
+    lead = extended.shape[0] - rows
+    before_rows = tail_in[tail - lead :, :].astype(jnp.float32)
+    extended[0:lead, :] = jnp.where(s > 0, before_rows, 0.0)
+    extended[lead:, :] = inner_sig[...].astype(jnp.float32)
+    tap_count = taps_ref.shape[0]
+    convolved = jnp.zeros((rows, local), jnp.float32)
+    for position in range(tap_count):
+        offset = lead - (tap_count - 1) + position
+        convolved = convolved + taps_ref[position : position + 1, :] * extended[
+            offset : offset + rows, :
+        ]
+    conv_out[...] = (outer[...].astype(jnp.float32) * convolved).astype(jnp.bfloat16)
+
+    keep.wait()
+    keep_q.wait()
+    for k in range(1, heads):
+        c = order[k]
+        arrived(q_all.at[c], q_r.at[c])
+    for k in range(heads):
+        if k + 2 < heads:
+            forward_stage(k + 2)
+        if k + 1 < heads:
+            forward_square(k + 1)
+        finish_plane(k)
+        attend_plane(k)
+        if k == 0:
+            weight_copies[len(sources)].wait()
+            conv_part[...] = jnp.dot(
+                conv_out[...], wc_vmem[...], preferred_element_type=jnp.float32
+            )
+
+    lam = lambdas_ref[plane]
+    own_gain = head_gain_ref[:, pl.ds(pl.multiple_of(plane * lanes, lanes), lanes)]
+    column = lax.broadcasted_iota(jnp.int32, (rows, lanes), 1)
+    keep_o = pltpu.make_async_copy(o_send.at[plane], o_all.at[plane], local_sem.at[2])
+    keep_lt = pltpu.make_async_copy(lt_send.at[plane], lt_all.at[plane], local_sem.at[3])
+    for step in list(range(1, heads)) + [0]:
+        target = lax.rem(plane + step, heads)
+        maps = []
+        logs = []
+        for m in range(2):
+            held = accum[2 * target + m]
+            total = held[:, lanes:]
+            maps.append(held[:, :lanes] / total)
+            logs.append(jnp.log(total) + row_max[2 * target + m] * math.log(2.0))
+        diff = maps[0] - lam * maps[1]
+        mean = jnp.mean(diff * diff, axis=-1, keepdims=True)
+        o_send[target] = (diff * lax.rsqrt(mean + 1e-05) * own_gain).astype(jnp.bfloat16)
+        turned = jnp.where(column == 0, logs[0], logs[1]).T
+        lt_send[target] = turned[: lt_send.shape[1], :]
+        if step == 0:
+            keep_o.start()
+            keep_lt.start()
+        else:
+            device = at(target * RELAY + member)
+            launch(remote(o_send.at[target], o_all.at[plane], o_s.at[step], o_r.at[plane], device))
+            launch(
+                remote(lt_send.at[target], lt_all.at[plane], lt_s.at[step], lt_r.at[plane], device)
+            )
+    keep_o.wait()
+    keep_lt.wait()
+    for step in range(1, heads):
+        source = lax.rem(plane + step, heads)
+        arrived(o_all.at[source], o_r.at[source])
+        arrived(lt_all.at[source], lt_r.at[source])
+    for h in range(heads):
+        totals_ref[h] = lt_all[h, 0:2, :]
+        part = slice(h * lanes, (h + 1) * lanes)
+        opened = gate[:, part].astype(jnp.float32)
+        opened = opened / (1.0 + jnp.exp(-opened))
+        head_out[:, part] = (o_all[h].astype(jnp.float32) * opened).astype(jnp.bfloat16)
+    weight_copies[len(sources) + 1].wait()
+
+    def partial_rows(which):
+        there = pl.ds(pl.multiple_of(which * half_rows, half_rows), half_rows)
+        attn = jnp.dot(head_out[there, :], wo_vmem[...], preferred_element_type=jnp.float32)
+        return (attn + conv_part[there, :]).astype(jnp.bfloat16)
+
+    part_send[...] = partial_rows(1 - t)
+    exchange = remote(part_send, part_recv, part_sem.at[0], part_sem.at[1], at(s, 1 - t))
+    exchange.start()
+    own_rows = partial_rows(t).astype(jnp.float32)
+    exchange.wait()
+    mixed_ref[...] = (own_rows + part_recv[...].astype(jnp.float32)).astype(jnp.bfloat16)
+    for copy in started:
+        copy.wait_send()
+
+
+def fused(sp_count, *args):
+    tokens, norm_gain, wq = args[0], args[1], args[2]
+    lambdas, head_gain = args[10], args[11]
+    rows, half = tokens.shape
+    heads = lambdas.shape[0]
+    local = wq.shape[1]
+    lanes = local // heads
+    out_width = args[12].shape[1]
+    bf16, f32 = jnp.bfloat16, jnp.float32
+    vmem = pl.BlockSpec(memory_space=pltpu.VMEM)
+    hbm = pl.BlockSpec(memory_space=pl.ANY)
+    dma = pltpu.SemaphoreType.DMA
+    operands = list(args)
+    operands[1] = norm_gain.reshape(1, -1)
+    operands[11] = head_gain.reshape(1, -1)
+    return pl.pallas_call(
+        functools.partial(fused_kernel, sp_count, heads),
+        out_shape=(
+            jax.ShapeDtypeStruct((rows // 2, out_width), bf16),
+            jax.ShapeDtypeStruct((heads, 2, rows), f32),
+        ),
+        in_specs=[vmem, vmem]
+        + [hbm] * 7
+        + [vmem, pl.BlockSpec(memory_space=pltpu.SMEM), vmem, hbm, hbm],
+        out_specs=(vmem, vmem),
+        scratch_shapes=[
+            pltpu.VMEM((rows, half), bf16),
+            pltpu.VMEM((rows, 2 * half), bf16),
+            pltpu.VMEM((7,) + wq.shape, bf16),
+            pltpu.VMEM(args[12].shape, bf16),
+            pltpu.VMEM(args[13].shape, bf16),
+            pltpu.VMEM((heads, rows, 2 * lanes), bf16),
+            pltpu.VMEM((heads, rows, lanes), bf16),
+            pltpu.VMEM((sp_count, rows, 2 * lanes), bf16),
+            pltpu.VMEM((heads, rows, lanes), bf16),
+            pltpu.VMEM((2 * heads, rows, lanes), f32),
+            pltpu.VMEM((2 * heads, rows, 2 * lanes), f32),
+            pltpu.VMEM((rows, local), bf16),
+            pltpu.VMEM((rows, local), bf16),
+            pltpu.VMEM((rows, local), bf16),
+            pltpu.VMEM((16, local), bf16),
+            pltpu.VMEM((rows + 8, local), f32),
+            pltpu.VMEM((rows, local), bf16),
+            pltpu.VMEM((rows, local), bf16),
+            pltpu.VMEM((rows, out_width), f32),
+            pltpu.VMEM((heads, rows, lanes), bf16),
+            pltpu.VMEM((heads, rows, lanes), bf16),
+            pltpu.VMEM((heads, 8, rows), f32),
+            pltpu.VMEM((heads, 8, rows), f32),
+            pltpu.VMEM((rows // 2, out_width), bf16),
+            pltpu.VMEM((rows // 2, out_width), bf16),
+            dma((9,)),
+            dma((2,)),
+            dma((2,)),
+            dma((2,)),
+        ]
+        + [dma((heads,)) for _ in range(16)]
+        + [dma((4,))],
+        compiler_params=pltpu.CompilerParams(
+            collective_id=0, has_side_effects=True, vmem_limit_bytes=60 * 1024 * 1024
+        ),
+    )(*operands)
+
+
+def fits_square(mesh, heads, rows, key_columns, value_columns):
+    return (
+        mesh.shape["tp"] == 2
+        and mesh.shape["sp"] == heads * RELAY
+        and heads > 1
+        and rows % 32 == 0
+        and key_columns == value_columns == heads * 128
+    )
+
+
 def solution(mesh):
     placed = (
         P("sp", "tp"),
@@ -176,8 +625,15 @@
         P("tp", None),
         P("tp", None),
     )
+
+    def step(*args):
+        heads = args[10].shape[0]
+        if fits_square(mesh, heads, args[0].shape[0], args[2].shape[1], args[4].shape[1]):
+            return fused(mesh.shape["sp"], *args)
+        return per_device(*args)
+
     return jax.shard_map(
-        per_device,
+        step,
         mesh=mesh,
         in_specs=placed,
         out_specs=(P(("sp", "tp"), None), P("tp", None, "sp")),

time: 292 us -> 60.5 us (0.21)
  waiting for transfers between devices: 162 us -> 0 us
  local copies, waits for them, and re-layouts: 73.4 us -> 3.18 us
  Pallas kernels: 0 us -> 56.2 us
  matrix products: 18.8 us -> 0 us
  between operations: 14 us -> 0.64 us
  loops' own time: 11 us -> 0 us
  other arithmetic: 5.93 us -> 0 us
  starting transfers between devices: 4.27 us -> 0 us
    all_gather x3 -> x0, waiting for transfers between devices: 112 us -> none  [the longest x1 69.5 us: per_device(): key_piece = lax.all_gather(key, 'sp', axis=0, tiled=True)]
    pallas_call x0 -> x1, Pallas kernels: none -> 56.2 us  [fused(): pl.pallas_call(functools.partial(fused_kernel, sp_count, heads), out_shap...]
    reduce_scatter x1 -> x0, waiting for transfers between devices: 47.8 us -> none  [per_device(): lax.psum_scatter((jnp.dot(head_out, attn_out_weight, preferred_element_ty...]
    while x2 -> x0, local copies, waits for them, and re-layouts: 25.2 us -> none  [per_device(): lax.scan(one_block, carry, (key_blocks, value_blocks, jnp.arange(length /...]
    reshape x2 -> x0, local copies, waits for them, and re-layouts: 23 us -> none  [the longest x1 16.1 us: per_device(): key_piece.reshape(length // block_len, block_len, head_count, 2, key_size)]
    dot_general x5 -> x0, matrix products: 18.8 us -> none  [the longest x1 9.46 us: per_device(): raw = jnp.dot(normed_piece, joined, preferred_element_type=jnp.float32)]
    another operation x9 -> x0, loops' own time: 11 us -> none  [the longest x1 10.8 us: per_device(): lax.scan(one_block, carry, (key_blocks, value_blocks, jnp.arange(length /...]
    unnamed x34 -> x2, local copies, waits for them, and re-layouts: 12.1 us -> 3.18 us
  transfers between devices with their start and end apart: 5 -> 0, of which waited for: 5 -> 0; matrix products, arithmetic and copies ran while one was open for 18% -> 0% of each run, Pallas kernels for 0% -> 0%
where the time goes in v1:
time: 60.5 us; the launch traced here: 60 us
  Pallas kernels  56.2 us (93%)
  local copies, waits for them, and re-layouts  3.18 us (5%)
  between operations  0.64 us (1%)
    pallas_call x1, Pallas kernels, fused(): pl.pallas_call(functools.partial(fused_kernel, sp_count, heads), out_shap...  56.2 us
    unnamed x2, local copies, waits for them, and re-layouts  3.18 us

profile of v1, /device:TPU:0, one launch (start us, length us, event | category | flops | bytes accessed | tf_op | source)
XLA Modules:
  0.0 60.0 jit_solution(3195156483517193412)
XLA Ops:
  0.6 56.2 %shard_map.149 = (bf16[128,2048]{1,0:T(8,128)(2,1)}, f32[4,2,256]{2,1,0:T(2,128)}) custom-call(bf16[256,1024]{1,0:T(8,128)(2,1)} %tokens_ref.1, f32[1,2048]{1,0:T(1,128)} %bitcast.2, bf16[2048,512]{1,0:T(8,128)(2,1)} %wq_hbm.1, bf16[2048,512]{1,0:T(8,128)(2,1)} %wk_hbm.1, bf16[2048,512]{1,0:T(8,128)(2,1)} %wv_hbm.1, bf16[2048,512]{1,0:T(8,128)(2,1)} %wg_hbm.1, ...), custom_call_target="tpu_custom_call" | custom-call | tf_op jit(solution)/shard_map/pallas_call | solution.py:552
  56.8 1.9 %copy.18 = bf16[128,2048]{1,0:T(8,128)(2,1)} copy(bf16[128,2048]{1,0:T(8,128)(2,1)} %get-tuple-element.4) | data formatting | bytes 1048576
  58.7 1.3 %copy.19 = f32[4,2,256]{2,1,0:T(2,128)} copy(f32[4,2,256]{2,1,0:T(2,128)} %get-tuple-element.5) | data formatting | bytes 16384

commit v2 on v1

--- a/solution.py
+++ b/solution.py
@@ -430,60 +430,50 @@
                 weights, values, preferred_element_type=jnp.float32
             )
 
-    def attend_plane(k):
-        c = order[k]
-        attend(c, c, True)
-
+    def attend_same(k):
+        attend(order[k], order[k], True)
+
+    def attend_later(k):
         for qi in range(1, heads):
 
-            @pl.when(qi > c)
+            @pl.when(qi > order[k])
             def _(qi=qi):
-                attend(qi, c, False)
-
-    forward_stage(1)
-    forward_square(0)
+                attend(qi, order[k], False)
+
     outer[...] = project(5)
     gate[...] = project(6)
 
-    arrived(tail_in, tail_sem.at[1])
-    lead = extended.shape[0] - rows
-    before_rows = tail_in[tail - lead :, :].astype(jnp.float32)
-    extended[0:lead, :] = jnp.where(s > 0, before_rows, 0.0)
-    extended[lead:, :] = inner_sig[...].astype(jnp.float32)
-    tap_count = taps_ref.shape[0]
-    convolved = jnp.zeros((rows, local), jnp.float32)
-    for position in range(tap_count):
-        offset = lead - (tap_count - 1) + position
-        convolved = convolved + taps_ref[position : position + 1, :] * extended[
-            offset : offset + rows, :
-        ]
-    conv_out[...] = (outer[...].astype(jnp.float32) * convolved).astype(jnp.bfloat16)
-
-    keep.wait()
-    keep_q.wait()
-    for k in range(1, heads):
-        c = order[k]
-        arrived(q_all.at[c], q_r.at[c])
-    for k in range(heads):
-        if k + 2 < heads:
-            forward_stage(k + 2)
-        if k + 1 < heads:
-            forward_square(k + 1)
-        finish_plane(k)
-        attend_plane(k)
-        if k == 0:
-            weight_copies[len(sources)].wait()
-            conv_part[...] = jnp.dot(
-                conv_out[...], wc_vmem[...], preferred_element_type=jnp.float32
-            )
+    def mix_conv():
+        arrived(tail_in, tail_sem.at[1])
+        lead = extended.shape[0] - rows
+        before_rows = tail_in[tail - lead :, :].astype(jnp.float32)
+        extended[0:lead, :] = jnp.where(s > 0, before_rows, 0.0)
+        extended[lead:, :] = inner_sig[...].astype(jnp.float32)
+        tap_count = taps_ref.shape[0]
+        convolved = jnp.zeros((rows, local), jnp.float32)
+        for position in range(tap_count):
+            offset = lead - (tap_count - 1) + position
+            convolved = convolved + taps_ref[position : position + 1, :] * extended[
+                offset : offset + rows, :
+            ]
+        conv_out[...] = (outer[...].astype(jnp.float32) * convolved).astype(jnp.bfloat16)
+        weight_copies[len(sources)].wait()
+        conv_part[...] = jnp.dot(conv_out[...], wc_vmem[...], preferred_element_type=jnp.float32)
 
     lam = lambdas_ref[plane]
     own_gain = head_gain_ref[:, pl.ds(pl.multiple_of(plane * lanes, lanes), lanes)]
     column = lax.broadcasted_iota(jnp.int32, (rows, lanes), 1)
     keep_o = pltpu.make_async_copy(o_send.at[plane], o_all.at[plane], local_sem.at[2])
     keep_lt = pltpu.make_async_copy(lt_send.at[plane], lt_all.at[plane], local_sem.at[3])
-    for step in list(range(1, heads)) + [0]:
-        target = lax.rem(plane + step, heads)
+
+    def returns(target):
+        device = at(target * RELAY + member)
+        return (
+            remote(o_send.at[target], o_all.at[plane], o_s.at[target], o_r.at[plane], device),
+            remote(lt_send.at[target], lt_all.at[plane], lt_s.at[target], lt_r.at[plane], device),
+        )
+
+    def give_back(target):
         maps = []
         logs = []
         for m in range(2):
@@ -496,15 +486,40 @@
         o_send[target] = (diff * lax.rsqrt(mean + 1e-05) * own_gain).astype(jnp.bfloat16)
         turned = jnp.where(column == 0, logs[0], logs[1]).T
         lt_send[target] = turned[: lt_send.shape[1], :]
-        if step == 0:
+
+        @pl.when(plane == target)
+        def _():
             keep_o.start()
             keep_lt.start()
-        else:
-            device = at(target * RELAY + member)
-            launch(remote(o_send.at[target], o_all.at[plane], o_s.at[step], o_r.at[plane], device))
-            launch(
-                remote(lt_send.at[target], lt_all.at[plane], lt_s.at[step], lt_r.at[plane], device)
-            )
+
+        @pl.when(plane != target)
+        def _():
+            for copy in returns(target):
+                copy.start()
+
+    if heads > 1:
+        forward_stage(1)
+    forward_square(0)
+    keep.wait()
+    keep_q.wait()
+    finish_plane(0)
+    attend_same(0)
+    for k in range(1, heads):
+        if k + 1 < heads:
+            forward_stage(k + 1)
+        forward_square(k)
+    for k in range(1, heads):
+        c = order[k]
+        arrived(q_all.at[c], q_r.at[c])
+    attend_later(0)
+    for k in range(1, heads):
+        finish_plane(k)
+        attend_same(k)
+        attend_later(k)
+        give_back(k - 1)
+        if k == 1:
+            mix_conv()
+    give_back(heads - 1)
     keep_o.wait()
     keep_lt.wait()
     for step in range(1, heads):
@@ -532,6 +547,12 @@
     mixed_ref[...] = (own_rows + part_recv[...].astype(jnp.float32)).astype(jnp.bfloat16)
     for copy in started:
         copy.wait_send()
+    for target in range(heads):
+
+        @pl.when(plane != target)
+        def _(target=target):
+            for copy in returns(target):
+                copy.wait_send()
 
 
 def fused(sp_count, *args):

time: 60.5 us -> 62.1 us (1.026)
  the two profiles are of different devices: /device:TPU:0 before, /device:TPU:17 now
where the time goes in v2:
time: 62.1 us; the launch traced here: 61.9 us
  Pallas kernels  58.1 us (94%)
  local copies, waits for them, and re-layouts  3.18 us (5%)
  between operations  0.64 us (1%)
    pallas_call x1, Pallas kernels, fused(): pl.pallas_call(functools.partial(fused_kernel, sp_count, heads), out_shap...  58.1 us
    unnamed x2, local copies, waits for them, and re-layouts  3.18 us

profile of v2, /device:TPU:17, one launch (start us, length us, event | category | flops | bytes accessed | tf_op | source)
XLA Modules:
  0.0 61.9 jit_solution(15902619626499127725)
XLA Ops:
  0.6 58.1 %shard_map.149 = (bf16[128,2048]{1,0:T(8,128)(2,1)}, f32[4,2,256]{2,1,0:T(2,128)}) custom-call(bf16[256,1024]{1,0:T(8,128)(2,1)} %tokens_ref.1, f32[1,2048]{1,0:T(1,128)} %bitcast.2, bf16[2048,512]{1,0:T(8,128)(2,1)} %wq_hbm.1, bf16[2048,512]{1,0:T(8,128)(2,1)} %wk_hbm.1, bf16[2048,512]{1,0:T(8,128)(2,1)} %wv_hbm.1, bf16[2048,512]{1,0:T(8,128)(2,1)} %wg_hbm.1, ...), custom_call_target="tpu_custom_call" | custom-call | tf_op jit(solution)/shard_map/pallas_call | solution.py:573
  58.7 1.9 %copy.18 = bf16[128,2048]{1,0:T(8,128)(2,1)} copy(bf16[128,2048]{1,0:T(8,128)(2,1)} %get-tuple-element.4) | data formatting | bytes 1048576
  60.6 1.3 %copy.19 = f32[4,2,256]{2,1,0:T(2,128)} copy(f32[4,2,256]{2,1,0:T(2,128)} %get-tuple-element.5) | data formatting | bytes 16384
